TPU v7x, 512 devices: a whole 4x8x8 slice. The times are simulated.
512 devices in a mesh: sp: 64 (over z, y), tp: 8 (over x, core).
Axes of the slice: x: 4, y: 8, z: 8, core: 2. Of those that a mesh axis runs over, the one named last changes fastest.
Arguments:
- value_in: bfloat16 [23040, 2048], P('sp', 'tp'), may hold values from -240 to 240
- gate_in: bfloat16 [23040, 2048], P('sp', 'tp'), may hold values from -8 to 8
- taps: float32 [31, 2048], P(None, 'tp'), may hold values from -1 to 1
- norm_gain: float32 [2048], P('tp'), may hold values from 0.1 to 1.9
- norm_bias: float32 [2048], P('tp'), may hold values from -3 to 3
- proj_weight: bfloat16 [2048, 4096], P('tp', 'sp'), may hold values from -0.125 to 0.125
- out_grad: bfloat16 [23040, 4096], P('sp'), may hold values from -16 to 16
Outputs:
- value_grad: bfloat16 [23040, 2048], P('sp', 'tp')
- gate_grad: bfloat16 [23040, 2048], P('sp', 'tp')
- tap_grad: float32 [31, 2048], P(None, 'tp')
- gain_grad: float32 [2048], P('tp')
- bias_grad: float32 [2048], P('tp')
- weight_grad: float32 [2048, 4096], P('tp', 'sp')
All inputs are finite; a program needn't handle non-finite values.
Results may differ from a plain program's by a relative error of at most 0.0051.
Values may be sent and summed in bfloat16 or wider, within the bound.
A program may use at most 64 MiB of HBM per device.

v0:
```python
import functools
import jax
import jax.numpy as jnp
from jax import lax
from jax.sharding import Mesh
from jax.sharding import PartitionSpec as P

SP = ("sp_0", "sp_1")


def padded_2(cells, sides, width):
    for axis, dim in sides:
        count = lax.axis_size(axis)
        ends = count - 1
        head = lax.slice_in_dim(cells, 0, width, axis=dim)
        tail = lax.slice_in_dim(cells, cells.shape[dim] - width, cells.shape[dim], axis=dim)
        cells = jnp.concatenate(
            [
                lax.ppermute(tail, axis, [(i, (i + 1) % count) for i in range(ends)]),
                cells,
                lax.ppermute(head, axis, [((i + 1) % count, i) for i in range(ends)]),
            ],
            axis=dim,
        )
    return cells


def copy_for_each(value, axis):
    copies = jnp.broadcast_to(value, (lax.axis_size(axis), *value.shape))
    return lax.all_to_all(copies, axis, split_axis=0, concat_axis=0, tiled=True)


def of_everyone(value, axis):
    everything = copy_for_each(value, axis)
    return jnp.sum(everything, axis=0)


def together(arrays, axis):
    flat, at, finished = (jnp.concatenate([a.reshape(-1) for a in arrays]), 0, [])
    subtotal = of_everyone(flat, axis)
    for a in arrays:
        finished.append(subtotal[at : at + a.size].reshape(a.shape))
        at += a.size
    return tuple(finished)


def in_order(tiles, dim):
    tiles = jnp.moveaxis(tiles, 0, dim)
    lengths = tiles.shape
    return tiles.reshape(*lengths[:dim], lengths[dim] * lengths[dim + 1], *lengths[dim + 2 :])


def stacked_from(value, axes, order):
    tiles = value[None]
    for k in order:
        tiles = lax.all_gather(tiles, axes[k], axis=0, tiled=True)
    held = [lax.axis_size(axes[k]) for k in reversed(order)]
    tiles = tiles.reshape(*held, *value.shape)
    turned = sorted(range(len(order)), key=lambda place: order[len(order) - 1 - place])
    return tiles.transpose(*turned, *range(len(order), tiles.ndim)).reshape(-1, *value.shape)


def gather_axes(value, axes, order, dim):
    return in_order(stacked_from(value, axes, order), dim)


def passed_along(block, axis, distance):
    devices = range(lax.axis_size(axis))
    route = [(i - distance, i) for i in devices if i - distance in devices]
    return lax.ppermute(block, axis, route)


def by_axis(value, axes):
    return functools.reduce(lax.psum, axes, value)


def summed_rows(subtotal, axes):
    for axis in axes:
        subtotal = lax.psum_scatter(subtotal, axis, scatter_dimension=0, tiled=True)
    return subtotal


def on_device(value_in, gate_in, taps, norm_gain, norm_bias, proj_weight, out_grad):
    f32 = jnp.float32
    rows = value_in.shape[0]
    local_width = value_in.shape[1]
    span = taps.shape[0]
    half = span // 2
    width_all = local_width * lax.axis_size("tp")
    gate_sig = jax.nn.sigmoid(gate_in.astype(f32))
    value_f = value_in.astype(f32)
    mixed = (value_f * gate_sig).astype(jnp.bfloat16)
    padded = padded_2(mixed, ((SP, 0),), half).astype(f32)
    conv = jnp.zeros((rows, local_width), f32)
    for k in range(span):
        conv = conv + taps[k] * padded[k : k + rows]
    total, squares = together((jnp.sum(conv, axis=1), jnp.sum(conv * conv, axis=1)), "tp")
    mean = total / width_all
    centred = conv - mean[:, None]
    spread = squares / width_all - mean * mean
    inv = lax.rsqrt(spread + 1e-06)
    normed = centred * inv[:, None]
    pre = normed * norm_gain + norm_bias
    act = jax.nn.silu(pre).astype(jnp.bfloat16)
    columns = out_grad
    act_grad = lax.dot_general(
        columns,
        gather_axes(proj_weight, SP, (0, 1), 1),
        (((1,), (1,)), ((), ())),
        preferred_element_type=f32,
    )
    sig_pre = jax.nn.sigmoid(pre)
    pre_grad = act_grad * sig_pre * (1.0 + pre * (1.0 - sig_pre))
    normed_grad = pre_grad * norm_gain
    first, second = together(
        (jnp.sum(normed_grad, axis=1), jnp.sum(normed_grad * normed, axis=1)), "tp"
    )
    conv_grad = inv[:, None] * (
        normed_grad - first[:, None] / width_all - normed * second[:, None] / width_all
    )
    local_pad = jnp.pad(conv_grad, ((2 * half, 2 * half), (0, 0)))
    spread_out = jnp.zeros((rows + 2 * half, local_width), f32)
    for k in range(span):
        spread_out = spread_out + taps[k] * local_pad[2 * half - k : 2 * half - k + rows + 2 * half]
    own_part = spread_out[half : half + rows]
    from_left = passed_along(spread_out[rows + half :], SP, 1)
    from_right = passed_along(spread_out[:half], SP, -1)
    mixed_grad = own_part.at[:half].add(from_left).at[rows - half :].add(from_right)
    tap_local = jnp.stack([jnp.sum(conv_grad * padded[k : k + rows], axis=0) for k in range(span)])
    gain_local = jnp.sum(pre_grad * normed, axis=0)
    bias_local = jnp.sum(pre_grad, axis=0)
    tap_grad, gain_grad, bias_grad = (
        by_axis(tap_local, SP),
        by_axis(gain_local, SP),
        by_axis(bias_local, SP),
    )
    value_grad = (mixed_grad * gate_sig).astype(jnp.bfloat16)
    gate_grad = (mixed_grad * value_f * gate_sig * (1.0 - gate_sig)).astype(jnp.bfloat16)
    columns = out_grad
    summed = summed_rows(
        lax.dot_general(columns, act, (((0,), (0,)), ((), ())), preferred_element_type=f32), SP
    )
    weight_grad = jnp.transpose(summed)
    return (value_grad, gate_grad, tap_grad, gain_grad, bias_grad, weight_grad)


def solution(mesh):
    finer = Mesh(mesh.devices.reshape(8, 8, mesh.shape["tp"]), ("sp_0", "sp_1", "tp"))
    in_specs = (P(SP, "tp"), P(SP, "tp"), P(None, "tp"), P("tp"), P("tp"), P("tp", SP), P(SP, None))
    out_specs = (P(SP, "tp"), P(SP, "tp"), P(None, "tp"), P("tp"), P("tp"), P("tp", SP))
    return jax.shard_map(
        on_device, mesh=finer, in_specs=in_specs, out_specs=out_specs, check_vma=False
    )
```

profile of v0, /device:TPU:4, one launch (start us, length us, event | category | flops | bytes accessed | tf_op | source)
XLA Modules:
  0.0 201.0 jit_solution(267206037773052146)
XLA Ops:
  8.1 31.5 %all-gather = bf16[2048,64]{0,1:T(8,128)(2,1)S(1)} all-gather(bf16[256,64]{0,1:T(8,128)(2,1)} %param.16), channel_id=2, replica_groups=mesh['sp_0'=8,'sp_1'=8,'tp'=8] {'sp_0'}, dimensions={0}, use_global_device_ids=true | all-gather | bytes 294912 | tf_op jit(solution)/shard_map/all_gather | solution.py:56
  40.4 1.1 fusion.62
  41.5 3.5 %collective-permute-start = (bf16[15,256]{1,0:T(8,128)(2,1)S(1)}, bf16[15,256]{1,0:T(8,128)(2,1)S(1)}, u32[]{:S(2)}, u32[]{:S(2)}) collective-permute-start(bf16[15,256]{1,0:T(8,128)(2,1)S(1)} %get-tuple-element.121), channel_id=1, source_target_pairs={{0,8},{8,16},{16,24},{24,32},{32,40},{40,48},{48,56},{56,64},{64,7... | collective-permute-start | bytes 23048 | tf_op jit(solution)/shard_map/ppermute | solution.py:19
  45.0 1.3 collective-permute-start.1
  46.3 1.0 fusion.75
  48.3 2.2 %collective-permute-done.1 = bf16[15,256]{1,0:T(8,128)(2,1)S(1)} collective-permute-done((bf16[15,256]{1,0:T(8,128)(2,1)S(1)}, bf16[15,256]{1,0:T(8,128)(2,1)S(1)}, u32[]{:S(2)}, u32[]{:S(2)}) %collective-permute-start.1) | collective-permute-done | bytes 7712 | tf_op jit(solution)/shard_map/ppermute | solution.py:21
  50.6 2.2 %fusion.72 = (f32[360]{0:T(512)S(1)}, f32[360]{0:T(512)S(1)}, f32[360,256]{1,0:T(8,128)}) fusion(f32[390,256]{1,0:T(8,128)S(1)} %maximum_convert_fusion, f32[256]{0:T(256)S(1)} %bitcast.144, f32[256]{0:T(256)S(1)} %bitcast.146, f32[256]{0:T(256)S(1)} %bitcast.88, f32[256]{0:T(256)S(1)} %bitcast.90, f32[256]{0:T(256)S(1)} %bitcast.92, f32[256]{0:T(256)S(1)} %bitcast.94, ...), kind=kLoop, calls=%fused_computation.158 | loop fusion | flops 5897520 | bytes 11831104 | tf_op jit(solution)/shard_map/reduce_sum | solution.py:97
  52.9 7.6 %all_to_all.12 = f32[8,1,720]{2,1,0:T(1,128)S(1)} all-to-all(f32[8,1,720]{2,1,0:T(1,128)S(1)} %broadcast_in_dim.6), channel_id=1, replica_groups=mesh['sp_0'=8,'sp_1'=8,'tp'=8] {'tp'}, dimensions={0} | all-to-all | bytes 46080 | tf_op jit(solution)/shard_map/all_to_all | solution.py:30
  60.6 4.4 %convolution_bitcast_fusion = f32[4096,256]{0,1:T(8,128)} fusion(bf16[360,4096]{1,0:T(8,128)(2,1)S(1)} %copy-done, f32[360,256]{1,0:T(8,128)} %get-tuple-element.116, f32[256]{0:T(256)S(1)} %copy-done.6, f32[256]{0:T(256)S(1)} %copy-done.5, f32[360]{0:T(512)S(1)} %get-tuple-element.157, f32[360]{0:T(512)S(1)} %get-tuple-element.156), kind=kOutput, calls=%fused_computation | convolution fusion | flops 755804160 | bytes 7516992 | tf_op jit(solution)/shard_map/dot_general | solution.py:141
  65.1 24.0 %all-gather.3.cloned.1.call-done = bf16[64,256,64]{1,0,2:T(8,128)(2,1)} async-done(((bf16[8,256,64]{1,0,2:T(8,128)(2,1)}), bf16[64,256,64]{1,0,2:T(8,128)(2,1)}) %all-gather.3.cloned.1.call-update) | async-done | bytes 2097168 | tf_op jit(solution)/shard_map/all_gather | solution.py:56
  89.0 2.8 %copy.28 = bf16[8,8,256,64]{2,3,1,0:T(8,128)(2,1)S(1)} copy(bf16[8,8,256,64]{2,0,1,3:T(8,128)(2,1)} %bitcast.82) | data formatting | bytes 4194304 | tf_op jit(solution)/shard_map/transpose | solution.py:60
  91.9 2.4 %multiply_reduce_fusion = (f32[256]{0:T(256)}, f32[360]{0:T(512)S(1)}, f32[360]{0:T(512)S(1)}, f32[256]{0:T(256)}, f32[360,256]{1,0:T(8,128)}) fusion(f32[360,256]{1,0:T(8,128)S(1)} %copy-done.1, f32[360]{0:T(512)S(1)} %get-tuple-element.157, f32[360]{0:T(512)S(1)} %get-tuple-element.156, f32[256]{0:T(256)S(1)} %copy-done.5, f32[256]{0:T(256)S(1)} %copy-done.6, ...), kind=kOutput, calls=%fused_computation.102 | convolution fusion | flops 756724480 | bytes 5793408 | tf_op jit(solution)/shard_map/dot_general | solution.py:106
  94.4 7.6 %all_to_all.13 = f32[8,1,720]{2,1,0:T(1,128)S(1)} all-to-all(f32[8,1,720]{2,1,0:T(1,128)S(1)} %broadcast_in_dim.8), channel_id=1, replica_groups=mesh['sp_0'=8,'sp_1'=8,'tp'=8] {'tp'}, dimensions={0} | all-to-all | bytes 46080 | tf_op jit(solution)/shard_map/all_to_all | solution.py:30
  102.0 2.6 %multiply_reduce_fusion.1 = (f32[256]{0:T(256)S(1)}, f32[256]{0:T(256)}, f32[256]{0:T(256)}, f32[256]{0:T(256)}, f32[256]{0:T(256)}, /*index=5*/f32[256]{0:T(256...) fusion(f32[390,256]{1,0:T(8,128)S(1)} %maximum_convert_fusion, ...), kind=kLoop, calls=%fused_computation.103 | loop fusion | flops 4050432 | bytes 7766656 | tf_op jit(solution)/shard_map/reduce_sum | solution.py:129
  105.3 1.2 fusion.55
  107.9 1.3 collective-permute-start.3
  109.2 5.1 %collective-permute-start.2 = (f32[15,256]{1,0:T(8,128)}, f32[15,256]{1,0:T(8,128)}, u32[]{:S(2)}, u32[]{:S(2)}) collective-permute-start(f32[15,256]{1,0:T(8,128)} %get-tuple-element.120), channel_id=1, source_target_pairs={{0,8},{8,16},{16,24},{24,32},{32,40},{40,48},{48,56},{56,64},{64,7... | collective-permute-start | bytes 46088 | tf_op jit(solution)/shard_map/ppermute | solution.py:70
  114.4 8.1 %reduce-scatter.5.cloned.1.call-done = f32[512,256]{0,1:T(8,128)} async-done(((f32[4096,256]{0,1:T(8,128)}), f32[512,256]{0,1:T(8,128)}) %reduce-scatter.5.cloned.1.call-update) | async-done | bytes 524304 | tf_op jit(solution)/shard_map/reduce_scatter | solution.py:79
  122.4 2.0 %copy.32 = f32[512,256]{1,0:T(8,128)} copy(f32[512,256]{0,1:T(8,128)} %reduce-scatter.5.cloned.1.call-done) | data formatting | bytes 1048576
  124.5 2.2 %multiply_reduce_fusion.19 = (f32[256]{0:T(256)}, f32[256]{0:T(256)}, f32[256]{0:T(256)}, f32[256]{0:T(256)}, f32[256]{0:T(256)}, /*index=5*/f32[256]{0:T(256)},...) fusion(f32[360,256]{1,0:T(8,128)} %copy-done.2, ...), kind=kLoop, calls=%fused_computation.121 | loop fusion | flops 2392832 | bytes 5174272 | tf_op jit(solution)/shard_map/reduce_sum | solution.py:129
  126.7 2.9 %stack.127 = f32[31,256]{1,0:T(8,128)S(1)} concatenate(f32[1,256]{1,0:T(1,128)} %bitcast.178, f32[1,256]{1,0:T(1,128)} %bitcast.177, f32[1,256]{1,0:T(1,128)} %bitcast.176, f32[1,256]{1,0:T(1,128)} %bitcast.175, f32[1,256]{1,0:T(1,128)} %bitcast.174, f32[1,256]{1,0:T(1,128)} %bitcast.173, f32[1,256]{1,0:T(1,128)} %bitcast.172, f32[1,256]{1,0:T(1,128)} %bitcast.171, ...), dimensions={0} | concatenate | bytes 63488 | tf_op jit(solution)/shard_map/stack | solution.py:129
  129.5 29.3 %all-reduce.2 = (f32[31,256]{1,0:T(8,128)S(1)}, f32[256]{0:T(256)S(1)}, f32[256]{0:T(256)S(1)}) all-reduce(f32[31,256]{1,0:T(8,128)S(1)} %stack.127, f32[256]{0:T(256)} %get-tuple-element.103, f32[256]{0:T(256)} %get-tuple-element.106), channel_id=1, replica_groups=mesh['sp_0'=8,'sp_1'=8,'tp'=8] {'sp_0'}, use_global_device_ids=true, to_apply=%region_37.38 | all-reduce | flops 8448 | bytes 67584 | tf_op jit(solution)/shard_map/psum | solution.py:74
  158.8 30.7 %all-reduce.1 = (f32[31,256]{1,0:T(8,128)}, f32[256]{0:T(256)}, f32[256]{0:T(256)}) all-reduce(f32[31,256]{1,0:T(8,128)S(1)} %get-tuple-element.112, f32[256]{0:T(256)S(1)} %get-tuple-element.113, f32[256]{0:T(256)S(1)} %get-tuple-element.114), channel_id=1, replica_groups=mesh['sp_0'=8,'sp_1'=8,'tp'=8] {'sp_1'}, use_global_device_ids=true, to_apply=%region_38.39 | all-reduce | flops 8448 | bytes 67584 | tf_op jit(solution)/shard_map/psum | solution.py:74
  191.7 1.8 fusion.65
  (42 shorter events, 6.7 us)
Async XLA Ops:
  8.0 52.6 %copy-start = (bf16[360,4096]{1,0:T(8,128)(2,1)S(1)}, bf16[360,4096]{1,0:T(8,128)(2,1)}, u32[]{:S(2)}) copy-start(bf16[360,4096]{1,0:T(8,128)(2,1)} %param.17) | copy-start | bytes 8847364
  8.0 81.0 %all-gather.3.cloned.1.call-start = ((), (), s32[]{:S(2)}) async-start(), calls=%async_computation.4 | async-start | bytes 2359296 | tf_op jit(solution)/shard_map/all_gather | solution.py:56
  40.3 82.1 %reduce-scatter.5.cloned.1.call-start = ((), (), s32[]{:S(2)}) async-start(), calls=%async_computation.5 | async-start | bytes 4718592 | tf_op jit(solution)/shard_map/reduce_scatter | solution.py:79
  41.5 6.8 %collective-permute-start = (bf16[15,256]{1,0:T(8,128)(2,1)S(1)}, bf16[15,256]{1,0:T(8,128)(2,1)S(1)}, u32[]{:S(2)}, u32[]{:S(2)}) collective-permute-start(bf16[15,256]{1,0:T(8,128)(2,1)S(1)} %get-tuple-element.121), channel_id=1, source_target_pairs={{0,8},{8,16},{16,24},{24,32},{32,40},{40,48},{48,56},{56,64},{64,7... | collective-permute-start | bytes 23048 | tf_op jit(solution)/shard_map/ppermute | solution.py:19
  45.0 5.5 %collective-permute-start.1 = (bf16[15,256]{1,0:T(8,128)(2,1)S(1)}, bf16[15,256]{1,0:T(8,128)(2,1)S(1)}, u32[]{:S(2)}, u32[]{:S(2)}) collective-permute-start(bf16[15,256]{1,0:T(8,128)(2,1)S(1)} %get-tuple-element.122), channel_id=1, source_target_pairs={{8,0},{16,8},{24,16},{32,24},{40,32},{48,40},{56,48},{64,56},{72,6... | collective-permute-start | bytes 23048 | tf_op jit(solution)/shard_map/ppermute | solution.py:21
  50.6 10.0 %copy-start.5 = (f32[256]{0:T(256)S(1)}, f32[256]{0:T(256)}, u32[]{:S(2)}) copy-start(f32[256]{0:T(256)} %param.14) | copy-start | bytes 3076
  50.6 10.0 %copy-start.6 = (f32[256]{0:T(256)S(1)}, f32[256]{0:T(256)}, u32[]{:S(2)}) copy-start(f32[256]{0:T(256)} %param.15) | copy-start | bytes 3076
  65.0 128.5 %reduce-scatter.7.cloned.1.call-start = ((), (), s32[]{:S(2)}) async-start(), calls=%async_computation.6 | async-start | bytes 589824
  89.0 2.8 %copy-start.1 = (f32[360,256]{1,0:T(8,128)S(1)}, f32[360,256]{1,0:T(8,128)}, u32[]{:S(2)}) copy-start(f32[360,256]{1,0:T(8,128)} %get-tuple-element.116) | copy-start | bytes 1105924
  104.6 0.7 copy-start.2
  106.6 0.8 copy-start.3
  107.9 83.6 %collective-permute-start.3 = (f32[15,256]{1,0:T(8,128)}, f32[15,256]{1,0:T(8,128)S(1)}, u32[]{:S(2)}, u32[]{:S(2)}) collective-permute-start(f32[15,256]{1,0:T(8,128)} %get-tuple-element.119), channel_id=1, source_target_pairs={{8,0},{16,8},{24,16},{32,24},{40,32},{48,40},{56,48},{64,56},{72,6... | collective-permute-start | bytes 46088 | tf_op jit(solution)/shard_map/ppermute | solution.py:70
  109.2 81.3 %collective-permute-start.2 = (f32[15,256]{1,0:T(8,128)}, f32[15,256]{1,0:T(8,128)}, u32[]{:S(2)}, u32[]{:S(2)}) collective-permute-start(f32[15,256]{1,0:T(8,128)} %get-tuple-element.120), channel_id=1, source_target_pairs={{0,8},{8,16},{16,24},{24,32},{32,40},{40,48},{48,56},{56,64},{64,7... | collective-permute-start | bytes 46088 | tf_op jit(solution)/shard_map/ppermute | solution.py:70
  124.5 67.2 %copy-start.4 = (bf16[360,256]{1,0:T(8,128)(2,1)S(1)}, bf16[360,256]{1,0:T(8,128)(2,1)}, u32[]{:S(2)}) copy-start(bf16[360,256]{1,0:T(8,128)(2,1)} %param.11) | copy-start | bytes 552964
Sparse Core Ops, SparseCore 0:
  40.5 48.5 all-gather.2
  124.6 38.2 reduce-scatter.6
Sparse Core Ops, SparseCore 1:
  65.1 57.3 reduce-scatter.4
where the time goes:
time: 202 us; the launch traced here: 201 us
  blocking collectives  107 us (53%)
  waiting for transfers between devices  34.3 us (17%)
  between operations  15.7 us (8%)
  local copies, waits for them, and re-layouts  14.1 us (7%)
  other arithmetic  12.2 us (6%)
  starting transfers between devices  11.3 us (6%)
  matrix products  6.77 us (3%)
    psum x2, blocking collectives, by_axis(): return functools.reduce(lax.psum, axes, value)  59.9 us
    all_gather x1, blocking collectives, stacked_from(): tiles = lax.all_gather(tiles, axes[k], axis=0, tiled=True)  31.5 us
    all_gather x1, waiting for transfers between devices, stacked_from(): tiles = lax.all_gather(tiles, axes[k], axis=0, tiled=True)  24 us
    all_to_all x2, blocking collectives, copy_for_each(): return lax.all_to_all(copies, axis, split_axis=0, concat_axis=0, tiled=True)  15.2 us
    reduce_scatter x1, waiting for transfers between devices, summed_rows(): subtotal = lax.psum_scatter(subtotal, axis, scatter_dimension=0, tiled=True)  8.09 us
    ppermute x2, starting transfers between devices, passed_along(): return lax.ppermute(block, axis, route)  6.43 us
    reduce_sum x2, other arithmetic, on_device(): jnp.sum(conv_grad * padded[k:k + rows], axis=0)  4.71 us
    dot_general x1, matrix products, on_device(): lax.dot_general(columns, act, (((0,), (0,)), ((), ())), preferred_element...  4.37 us
  transfers between devices with their start and end apart: 7, of which 3 were waited for; matrix products, arithmetic and copies ran while one was open for 15% of the time, Pallas kernels for 0%

commit v1 on v0

--- a/solution.py
+++ b/solution.py
@@ -53,7 +53,10 @@
 def stacked_from(value, axes, order):
     tiles = value[None]
     for k in order:
-        tiles = lax.all_gather(tiles, axes[k], axis=0, tiled=True)
+        size = lax.axis_size(axes[k])
+        blocks = jnp.stack([tiles for _ in range(size)])
+        blocks = lax.all_to_all(blocks, axes[k], split_axis=0, concat_axis=0)
+        tiles = jnp.concatenate(blocks, axis=0)
     held = [lax.axis_size(axes[k]) for k in reversed(order)]
     tiles = tiles.reshape(*held, *value.shape)
     turned = sorted(range(len(order)), key=lambda place: order[len(order) - 1 - place])

time: 202 us -> 213 us (1.054)
  the two profiles are of different devices: /device:TPU:4 before, /device:TPU:2 now
where the time goes in v1:
time: 213 us; the launch traced here: 212 us
  blocking collectives  152 us (71%)
  between operations  14.2 us (7%)
  local copies, waits for them, and re-layouts  12.4 us (6%)
  other arithmetic  12.4 us (6%)
  starting transfers between devices  11.3 us (5%)
  matrix products  6.78 us (3%)
  waiting for transfers between devices  2.27 us (1%)
    all_to_all x2, blocking collectives, stacked_from(): blocks = lax.all_to_all(blocks, axes[k], split_axis=0, concat_axis=0)  77 us
    psum x2, blocking collectives, by_axis(): return functools.reduce(lax.psum, axes, value)  57.7 us
    all_to_all x2, blocking collectives, copy_for_each(): return lax.all_to_all(copies, axis, split_axis=0, concat_axis=0, tiled=True)  17.7 us
    ppermute x2, starting transfers between devices, passed_along(): return lax.ppermute(block, axis, route)  6.42 us
    unnamed x17, local copies, waits for them, and re-layouts  5.09 us
    reduce_sum x2, other arithmetic, on_device(): jnp.sum(conv_grad * padded[k:k + rows], axis=0)  4.73 us
    dot_general x1, matrix products, on_device(): lax.dot_general(columns, act, (((0,), (0,)), ((), ())), preferred_element...  4.37 us
  transfers between devices with their start and end apart: 6, of which 1 were waited for; matrix products, arithmetic and copies ran while one was open for 10% of the time, Pallas kernels for 0%

profile of v1, /device:TPU:2, one launch (start us, length us, event | category | flops | bytes accessed | tf_op | source)
XLA Modules:
  0.0 211.9 jit_solution(3735356709747553879)
XLA Ops:
  7.2 1.3 fusion.62
  8.5 3.5 %collective-permute-start = (bf16[15,256]{1,0:T(8,128)(2,1)S(1)}, bf16[15,256]{1,0:T(8,128)(2,1)S(1)}, u32[]{:S(2)}, u32[]{:S(2)}) collective-permute-start(bf16[15,256]{1,0:T(8,128)(2,1)S(1)} %get-tuple-element.109), channel_id=1, source_target_pairs={{0,8},{8,16},{16,24},{24,32},{32,40},{40,48},{48,56},{56,64},{64,7... | collective-permute-start | bytes 23048 | tf_op jit(solution)/shard_map/ppermute | solution.py:19
  12.0 1.3 collective-permute-start.1
  13.3 1.0 fusion.75
  14.3 1.0 fusion.76
  15.3 2.2 %collective-permute-done.1 = bf16[15,256]{1,0:T(8,128)(2,1)S(1)} collective-permute-done((bf16[15,256]{1,0:T(8,128)(2,1)S(1)}, bf16[15,256]{1,0:T(8,128)(2,1)S(1)}, u32[]{:S(2)}, u32[]{:S(2)}) %collective-permute-start.1) | collective-permute-done | bytes 7712 | tf_op jit(solution)/shard_map/ppermute | solution.py:21
  17.6 2.2 %fusion.72 = (f32[360]{0:T(512)S(1)}, f32[360]{0:T(512)S(1)}, f32[360,256]{1,0:T(8,128)}) fusion(f32[390,256]{1,0:T(8,128)S(1)} %maximum_convert_fusion, f32[256]{0:T(256)S(1)} %bitcast.138, f32[256]{0:T(256)S(1)} %bitcast.140, f32[256]{0:T(256)S(1)} %bitcast.82, f32[256]{0:T(256)S(1)} %bitcast.84, f32[256]{0:T(256)S(1)} %bitcast.86, f32[256]{0:T(256)S(1)} %bitcast.88, ...), kind=kLoop, calls=%fused_computation.158 | loop fusion | flops 5897520 | bytes 11831104 | tf_op jit(solution)/shard_map/reduce_sum | solution.py:100
  19.9 10.0 %all_to_all.22 = f32[8,1,720]{2,1,0:T(1,128)S(1)} all-to-all(f32[8,1,720]{2,1,0:T(1,128)S(1)} %broadcast_in_dim.4), channel_id=1, replica_groups=mesh['sp_0'=8,'sp_1'=8,'tp'=8] {'tp'}, dimensions={0} | all-to-all | bytes 46080 | tf_op jit(solution)/shard_map/all_to_all | solution.py:30
  30.0 4.4 %convolution_bitcast_fusion = f32[4096,256]{0,1:T(8,128)} fusion(bf16[360,4096]{1,0:T(8,128)(2,1)S(1)} %copy-done, f32[360,256]{1,0:T(8,128)} %get-tuple-element.104, f32[256]{0:T(256)S(1)} %copy-done.7, f32[256]{0:T(256)S(1)} %copy-done.6, f32[360]{0:T(512)S(1)} %get-tuple-element.145, f32[360]{0:T(512)S(1)} %get-tuple-element.144), kind=kOutput, calls=%fused_computation | convolution fusion | flops 755804160 | bytes 7516992 | tf_op jit(solution)/shard_map/dot_general | solution.py:144
  35.2 22.6 %all_to_all.23 = bf16[8,1,256,64]{2,3,1,0:T(8,128)(2,1)S(1)} all-to-all(bf16[8,1,256,64]{2,3,1,0:T(8,128)(2,1)S(1)} %stack.102), channel_id=1, replica_groups=mesh['sp_0'=8,'sp_1'=8,'tp'=8] {'sp_0'}, dimensions={0} | all-to-all | bytes 524288 | tf_op jit(solution)/shard_map/all_to_all | solution.py:58
  58.1 54.4 %all_to_all.24 = bf16[8,8,256,64]{2,3,1,0:T(8,128)(2,1)S(1)} all-to-all(bf16[8,8,256,64]{2,3,1,0:T(8,128)(2,1)S(1)} %stack.103), channel_id=1, replica_groups=mesh['sp_0'=8,'sp_1'=8,'tp'=8] {'sp_1'}, dimensions={0} | all-to-all | bytes 4194304 | tf_op jit(solution)/shard_map/all_to_all | solution.py:58
  113.4 2.4 %multiply_reduce_fusion = (f32[256]{0:T(256)}, f32[360]{0:T(512)S(1)}, f32[360]{0:T(512)S(1)}, f32[256]{0:T(256)}, f32[360,256]{1,0:T(8,128)}) fusion(f32[360,256]{1,0:T(8,128)S(1)} %copy-done.1, f32[360]{0:T(512)S(1)} %get-tuple-element.145, f32[360]{0:T(512)S(1)} %get-tuple-element.144, f32[256]{0:T(256)S(1)} %copy-done.6, f32[256]{0:T(256)S(1)} %copy-done.7, ...), kind=kOutput, calls=%fused_computation.102 | convolution fusion | flops 756724480 | bytes 5793408 | tf_op jit(solution)/shard_map/dot_general | solution.py:109
  115.9 7.7 %all_to_all.25 = f32[8,1,720]{2,1,0:T(1,128)S(1)} all-to-all(f32[8,1,720]{2,1,0:T(1,128)S(1)} %broadcast_in_dim.5), channel_id=1, replica_groups=mesh['sp_0'=8,'sp_1'=8,'tp'=8] {'tp'}, dimensions={0} | all-to-all | bytes 46080 | tf_op jit(solution)/shard_map/all_to_all | solution.py:30
  123.8 2.6 %multiply_reduce_fusion.1 = (f32[256]{0:T(256)S(1)}, f32[256]{0:T(256)}, f32[256]{0:T(256)}, f32[256]{0:T(256)}, f32[256]{0:T(256)}, /*index=5*/f32[256]{0:T(256...) fusion(f32[390,256]{1,0:T(8,128)S(1)} %maximum_convert_fusion, ...), kind=kLoop, calls=%fused_computation.103 | loop fusion | flops 4050432 | bytes 7766656 | tf_op jit(solution)/shard_map/reduce_sum | solution.py:132
  127.1 1.2 fusion.55
  129.7 1.3 collective-permute-start.3
  131.0 5.1 %collective-permute-start.2 = (f32[15,256]{1,0:T(8,128)}, f32[15,256]{1,0:T(8,128)}, u32[]{:S(2)}, u32[]{:S(2)}) collective-permute-start(f32[15,256]{1,0:T(8,128)} %get-tuple-element.108), channel_id=1, source_target_pairs={{0,8},{8,16},{16,24},{24,32},{32,40},{40,48},{48,56},{56,64},{64,7... | collective-permute-start | bytes 46088 | tf_op jit(solution)/shard_map/ppermute | solution.py:73
  136.1 2.0 copy.24
  138.2 2.2 %multiply_reduce_fusion.19 = (f32[256]{0:T(256)}, f32[256]{0:T(256)}, f32[256]{0:T(256)}, f32[256]{0:T(256)}, f32[256]{0:T(256)}, /*index=5*/f32[256]{0:T(256)},...) fusion(f32[360,256]{1,0:T(8,128)} %copy-done.2, ...), kind=kLoop, calls=%fused_computation.121 | loop fusion | flops 2392832 | bytes 5174272 | tf_op jit(solution)/shard_map/reduce_sum | solution.py:132
  140.4 2.9 %stack.135 = f32[31,256]{1,0:T(8,128)S(1)} concatenate(f32[1,256]{1,0:T(1,128)} %bitcast.172, f32[1,256]{1,0:T(1,128)} %bitcast.171, f32[1,256]{1,0:T(1,128)} %bitcast.170, f32[1,256]{1,0:T(1,128)} %bitcast.169, f32[1,256]{1,0:T(1,128)} %bitcast.168, f32[1,256]{1,0:T(1,128)} %bitcast.167, f32[1,256]{1,0:T(1,128)} %bitcast.166, f32[1,256]{1,0:T(1,128)} %bitcast.165, ...), dimensions={0} | concatenate | bytes 63488 | tf_op jit(solution)/shard_map/stack | solution.py:132
  143.3 27.9 %all-reduce.2 = (f32[31,256]{1,0:T(8,128)S(1)}, f32[256]{0:T(256)S(1)}, f32[256]{0:T(256)S(1)}) all-reduce(f32[31,256]{1,0:T(8,128)S(1)} %stack.135, f32[256]{0:T(256)} %get-tuple-element.91, f32[256]{0:T(256)} %get-tuple-element.94), channel_id=1, replica_groups=mesh['sp_0'=8,'sp_1'=8,'tp'=8] {'sp_0'}, use_global_device_ids=true, to_apply=%region_37.38 | all-reduce | flops 8448 | bytes 67584 | tf_op jit(solution)/shard_map/psum | solution.py:77
  171.2 29.8 %all-reduce.1 = (f32[31,256]{1,0:T(8,128)}, f32[256]{0:T(256)}, f32[256]{0:T(256)}) all-reduce(f32[31,256]{1,0:T(8,128)S(1)} %get-tuple-element.100, f32[256]{0:T(256)S(1)} %get-tuple-element.101, f32[256]{0:T(256)S(1)} %get-tuple-element.102), channel_id=1, replica_groups=mesh['sp_0'=8,'sp_1'=8,'tp'=8] {'sp_1'}, use_global_device_ids=true, to_apply=%region_38.39 | all-reduce | flops 8448 | bytes 67584 | tf_op jit(solution)/shard_map/psum | solution.py:77
  201.0 1.0 slice.544
  203.2 1.8 fusion.65
  (43 shorter events, 5.8 us)
Async XLA Ops:
  7.2 22.9 %copy-start = (bf16[360,4096]{1,0:T(8,128)(2,1)S(1)}, bf16[360,4096]{1,0:T(8,128)(2,1)}, u32[]{:S(2)}) copy-start(bf16[360,4096]{1,0:T(8,128)(2,1)} %param.17) | copy-start | bytes 8847364
  7.2 129.0 %reduce-scatter.5.cloned.1.call-start = ((), (), s32[]{:S(2)}) async-start(), calls=%async_computation.6 | async-start | bytes 4718592 | tf_op jit(solution)/shard_map/reduce_scatter | solution.py:82
  8.5 6.8 %collective-permute-start = (bf16[15,256]{1,0:T(8,128)(2,1)S(1)}, bf16[15,256]{1,0:T(8,128)(2,1)S(1)}, u32[]{:S(2)}, u32[]{:S(2)}) collective-permute-start(bf16[15,256]{1,0:T(8,128)(2,1)S(1)} %get-tuple-element.109), channel_id=1, source_target_pairs={{0,8},{8,16},{16,24},{24,32},{32,40},{40,48},{48,56},{56,64},{64,7... | collective-permute-start | bytes 23048 | tf_op jit(solution)/shard_map/ppermute | solution.py:19
  12.0 5.5 %collective-permute-start.1 = (bf16[15,256]{1,0:T(8,128)(2,1)S(1)}, bf16[15,256]{1,0:T(8,128)(2,1)S(1)}, u32[]{:S(2)}, u32[]{:S(2)}) collective-permute-start(bf16[15,256]{1,0:T(8,128)(2,1)S(1)} %get-tuple-element.110), channel_id=1, source_target_pairs={{8,0},{16,8},{24,16},{32,24},{40,32},{48,40},{56,48},{64,56},{72,6... | collective-permute-start | bytes 23048 | tf_op jit(solution)/shard_map/ppermute | solution.py:21
  17.6 12.4 %copy-start.6 = (f32[256]{0:T(256)S(1)}, f32[256]{0:T(256)}, u32[]{:S(2)}) copy-start(f32[256]{0:T(256)} %param.14) | copy-start | bytes 3076
  17.6 12.4 %copy-start.7 = (f32[256]{0:T(256)S(1)}, f32[256]{0:T(256)}, u32[]{:S(2)}) copy-start(f32[256]{0:T(256)} %param.15) | copy-start | bytes 3076
  34.4 0.8 copy-start.5
  34.4 170.6 %reduce-scatter.7.cloned.1.call-start = ((), (), s32[]{:S(2)}) async-start(), calls=%async_computation.7 | async-start | bytes 589824
  112.4 1.0 copy-start.1
  126.4 0.7 copy-start.2
  128.3 0.8 copy-start.3
  129.7 73.3 %collective-permute-start.3 = (f32[15,256]{1,0:T(8,128)}, f32[15,256]{1,0:T(8,128)S(1)}, u32[]{:S(2)}, u32[]{:S(2)}) collective-permute-start(f32[15,256]{1,0:T(8,128)} %get-tuple-element.107), channel_id=1, source_target_pairs={{8,0},{16,8},{24,16},{32,24},{40,32},{48,40},{56,48},{64,56},{72,6... | collective-permute-start | bytes 46088 | tf_op jit(solution)/shard_map/ppermute | solution.py:73
  131.0 71.0 %collective-permute-start.2 = (f32[15,256]{1,0:T(8,128)}, f32[15,256]{1,0:T(8,128)}, u32[]{:S(2)}, u32[]{:S(2)}) collective-permute-start(f32[15,256]{1,0:T(8,128)} %get-tuple-element.108), channel_id=1, source_target_pairs={{0,8},{8,16},{16,24},{24,32},{32,40},{40,48},{48,56},{56,64},{64,7... | collective-permute-start | bytes 46088 | tf_op jit(solution)/shard_map/ppermute | solution.py:73
  138.2 65.0 %copy-start.4 = (bf16[360,256]{1,0:T(8,128)(2,1)S(1)}, bf16[360,256]{1,0:T(8,128)(2,1)}, u32[]{:S(2)}) copy-start(bf16[360,256]{1,0:T(8,128)(2,1)} %param.11) | copy-start | bytes 552964
Sparse Core Ops, SparseCore 0:
  34.5 61.9 reduce-scatter.4
  138.3 33.3 reduce-scatter.6
